TPU v7x, 32 devices: a whole 2x2x4 slice. The times are simulated.
32 devices in a mesh: ep: 4 (over y, x), tp: 8 (over z, core).
Axes of the slice: x: 2, y: 2, z: 4, core: 2. Of those that a mesh axis runs over, the one named last changes fastest.
Arguments:
- tokens: bfloat16 [64, 4096], P('ep'), may hold values from -6 to 6
- attn_gain: float32 [4096], replicated, may hold values from 0.1 to 1.9
- w_query: bfloat16 [4096, 2048], P('ep', 'tp'), may hold values from -0.15625 to 0.15625
- w_key: bfloat16 [4096, 2048], P('ep', 'tp'), may hold values from -0.09375 to 0.09375
- w_value: bfloat16 [4096, 2048], P('ep', 'tp'), may hold values from -0.09375 to 0.09375
- mix_lambda: float32 [16], P('tp'), may hold values from 0.3 to 0.8
- head_gain: float32 [128], replicated, may hold values from 0.1 to 1.9
- w_output: bfloat16 [2048, 4096], P('tp'), may hold values from -0.125 to 0.125
- cache_keys: bfloat16 [64, 1024, 2048], P('ep', None, 'tp'), may hold values from -180 to 180
- cache_value: bfloat16 [64, 1024, 2048], P('ep', None, 'tp'), may hold values from -6 to 6
- lengths: int32 [64], P('ep'), may hold values from 1 to 1024
- moe_gain: float32 [4096], replicated, may hold values from 0.1 to 1.9
- group_ids: int32 [64], P('ep'), may hold values from 0 to 1, as said below
- member_ids: int32 [64, 2], P('ep'), may hold values from 0 to 1, as said below
- group_gate: float32 [64], P('ep'), may hold values from 0.3 to 1
- member_logits: float32 [64, 2], P('ep'), may hold values from -4 to 4
- w_exp_gate: bfloat16 [4, 4096, 2048], P('ep', None, 'tp'), may hold values from -0.09375 to 0.09375
- w_exp_up: bfloat16 [4, 4096, 2048], P('ep', None, 'tp'), may hold values from -0.09375 to 0.09375
- w_exp_down: bfloat16 [4, 2048, 4096], P('ep', 'tp'), may hold values from -0.125 to 0.125
Outputs:
- mixed: bfloat16 [64, 4096], P('ep', 'tp')
- fresh_keys: bfloat16 [64, 2048], P('ep', 'tp')
- fresh_value: bfloat16 [64, 2048], P('ep', 'tp')
Inputs may be any that keep to these rules, and one draw needn't show every extreme that they name: `group_ids`: each index of ep holds 16 consecutive tokens, of which every group gets the same number. A token's 2 members differ, and every expert group_ids * 2 + member_ids receives exactly 8 of the token-expert pairs of each index of ep.
All inputs are finite; a program needn't handle non-finite values.
Results may differ from a plain program's by a relative error of at most 0.015.
The roundings to bfloat16 on the way count: a program that leaves them out, or rounds other values in their place, can miss the bound.
Values may be sent and summed in bfloat16 or wider, within the bound.
A program may use at most 64 MiB of HBM per device.

v0:
```python
import jax
import jax.numpy as jnp
from jax import lax
from jax.sharding import PartitionSpec as P

EPG = 2


EPS = 1e-06


def rms_scale(values, gain):
    return values * lax.rsqrt(jnp.mean(values * values, axis=-1, keepdims=True) + EPS) * gain


def on_device(
    tokens,
    attn_gain,
    w_query,
    w_key,
    w_value,
    mix_lambda,
    head_gain,
    w_output,
    cache_keys,
    cache_value,
    lengths,
    moe_gain,
    group_ids,
    member_ids,
    group_gate,
    member_logits,
    w_exp_gate,
    w_exp_up,
    w_exp_down,
):
    seqs, width = tokens.shape
    resid_in = tokens.astype(jnp.float32)
    normed = rms_scale(resid_in, attn_gain).astype(jnp.bfloat16)
    heads_local = mix_lambda.shape[0]
    qk_cols = w_query.shape[1]
    head_dim = qk_cols // (2 * heads_local)
    stacked = jnp.concatenate([w_query, w_key, w_value], axis=1)
    sliced = lax.all_to_all(normed, "ep", split_axis=1, concat_axis=0, tiled=True)
    projected = lax.psum_scatter(
        jnp.dot(sliced, stacked, preferred_element_type=jnp.float32),
        "ep",
        scatter_dimension=0,
        tiled=True,
    )
    projected = projected.astype(jnp.bfloat16)
    query = projected[:, :qk_cols]
    fresh_keys = projected[:, qk_cols : 2 * qk_cols]
    fresh_value = projected[:, 2 * qk_cols :]
    positions_all = cache_keys.shape[1]
    total_heads = heads_local * lax.axis_size("tp")
    head_index = (lax.axis_index("tp") * heads_local + jnp.arange(heads_local)).astype(jnp.float32)
    slopes = 2.0 ** (-8.0 * (head_index + 1.0) / total_heads)
    scale = head_dim ** (-0.5)
    positions = jnp.arange(positions_all)
    dist = (lengths[:, None] - positions[None, :]).astype(jnp.float32)
    valid = positions[None, :] < lengths[:, None]
    query4 = query.reshape(seqs, heads_local, 2, head_dim)
    keys5 = cache_keys.reshape(seqs, positions_all, heads_local, 2, head_dim)
    old = jnp.einsum("shcd,slhcd->cshl", query4, keys5, preferred_element_type=jnp.float32) * scale
    old = old - slopes[None, None, :, None] * dist[None, :, None, :]
    old = jnp.where(valid[None, :, None, :], old, -jnp.inf)
    fresh4 = fresh_keys.reshape(seqs, heads_local, 2, head_dim).astype(jnp.float32)
    new = jnp.moveaxis(jnp.sum(query4.astype(jnp.float32) * fresh4, axis=-1) * scale, 2, 0)
    full = jnp.concatenate([old, new[..., None]], axis=-1)
    maps = jax.nn.softmax(full, axis=-1)
    weights = (maps[0] - mix_lambda[None, :, None] * maps[1]).astype(jnp.bfloat16)
    values = cache_value.reshape(seqs, positions_all, heads_local, 2 * head_dim)
    head_mix = jnp.einsum(
        "shl,slhe->she", weights[..., :positions_all], values, preferred_element_type=jnp.float32
    )
    head_mix = head_mix + weights[..., positions_all].astype(jnp.float32)[
        ..., None
    ] * fresh_value.reshape(seqs, heads_local, 2 * head_dim).astype(jnp.float32)
    head_out = (
        rms_scale(head_mix, head_gain)
        .astype(jnp.bfloat16)
        .reshape(seqs, heads_local * 2 * head_dim)
    )
    term = jnp.dot(head_out, w_output, preferred_element_type=jnp.float32).astype(jnp.bfloat16)
    attn_sum = lax.psum(
        lax.optimization_barrier(term).astype(jnp.float32).astype(jnp.bfloat16), "tp"
    ).astype(jnp.float32)
    resid = resid_in + attn_sum
    moe_in = rms_scale(resid, moe_gain).astype(jnp.bfloat16)
    top = member_ids.shape[1]
    experts_local = w_exp_gate.shape[0]
    ep_count = lax.axis_size("ep")
    experts_all = experts_local * ep_count
    capacity = seqs * top // experts_all
    expert_ids = group_ids[:, None] * EPG + member_ids
    route_weight = jax.nn.softmax(member_logits, axis=-1) * group_gate[:, None]
    flat_ids = expert_ids.reshape(seqs * top)
    onehot = (flat_ids[:, None] == jnp.arange(experts_all)[None, :]).astype(jnp.int32)
    ranks = jnp.sum(jnp.cumsum(onehot, axis=0) * onehot, axis=1) - 1
    slot_grid = (flat_ids * capacity + ranks).reshape(seqs, top)
    slot_range = jnp.arange(experts_all * capacity)
    picker = jnp.sum((slot_grid[None, :, :] == slot_range[:, None, None]).astype(jnp.int32), axis=2)
    dispatch = jnp.dot(
        picker.astype(jnp.bfloat16), moe_in, preferred_element_type=jnp.float32
    ).astype(jnp.bfloat16)
    dispatch = dispatch.reshape(ep_count, experts_local, capacity, width)
    received = lax.all_to_all(dispatch, "ep", split_axis=0, concat_axis=2, tiled=True)
    received = received.reshape(experts_local, ep_count * capacity, width)
    gate = jnp.einsum("erd,edf->erf", received, w_exp_gate, preferred_element_type=jnp.float32)
    upper = jnp.einsum("erd,edf->erf", received, w_exp_up, preferred_element_type=jnp.float32)
    hidden = (jax.nn.silu(gate) * upper).astype(jnp.bfloat16)
    down = jnp.einsum("erf,efd->erd", hidden, w_exp_down, preferred_element_type=jnp.float32)
    summed = lax.psum_scatter(down.astype(jnp.bfloat16), "tp", scatter_dimension=2, tiled=True)
    cols = summed.shape[2]
    returned = lax.all_to_all(
        summed.reshape(experts_local, ep_count, capacity, cols),
        "ep",
        split_axis=1,
        concat_axis=0,
        tiled=True,
    )
    returned = returned.reshape(experts_all * capacity, cols)
    picked = returned[slot_grid].astype(jnp.float32)
    routed = jnp.sum(picked * route_weight[:, :, None], axis=1)
    own = lax.dynamic_slice_in_dim(resid, lax.axis_index("tp") * cols, cols, 1)
    mixed = (own + routed).astype(jnp.bfloat16)
    return (mixed, fresh_keys, fresh_value)


def solution(mesh):
    return jax.shard_map(
        on_device,
        mesh=mesh,
        in_specs=(
            P("ep", None),
            P(),
            P("ep", "tp"),
            P("ep", "tp"),
            P("ep", "tp"),
            P("tp"),
            P(),
            P("tp", None),
            P("ep", None, "tp"),
            P("ep", None, "tp"),
            P("ep"),
            P(),
            P("ep"),
            P("ep", None),
            P("ep"),
            P("ep", None),
            P("ep", None, "tp"),
            P("ep", None, "tp"),
            P("ep", "tp", None),
        ),
        out_specs=(P("ep", "tp"), P("ep", "tp"), P("ep", "tp")),
        check_vma=False,
    )
```

profile of v0, /device:TPU:0, one launch (start us, length us, event | category | flops | bytes accessed | tf_op | source)
XLA Modules:
  0.0 177.5 jit_solution(10258000634573673739)
XLA Ops:
  7.2 1.2 fusion.27
  8.4 1.0 fusion.29
  9.4 0.6 copy.110
  10.0 5.2 %all-to-all-start = ((bf16[16,4,1024]{2,0,1:T(8,128)(2,1)}), bf16[16,4,1024]{2,0,1:T(8,128)(2,1)S(1)}, u32[]{:S(2)}, u32[]{:S(2)}) async-start(bf16[16,4,1024]{2,0,1:T(8,128)(2,1)} %bitcast.80), calls=%async_computation | async-start | bytes 262144 | tf_op jit(solution)/shard_map/all_to_all | solution.py:44
  15.2 0.7 subtract_convert_fusion
  16.0 0.8 copy.78
  16.7 0.7 broadcast_multiply_fusion.1
  17.5 0.1 eq.28
  17.7 0.2 select_reduce_fusion
  17.9 0.1 sub.53
  18.0 0.1 compare_select_fusion
  18.0 2.2 %all-to-all-done = bf16[16,4,1024]{2,0,1:T(8,128)(2,1)S(1)} async-done(((bf16[16,4,1024]{2,0,1:T(8,128)(2,1)}), bf16[16,4,1024]{2,0,1:T(8,128)(2,1)S(1)}, u32[]{:S(2)}, u32[]{:S(2)}) %all-to-all-start) | async-done | bytes 131104 | tf_op jit(solution)/shard_map/all_to_all | solution.py:44
  20.3 2.5 %fusion.12 = f32[64,768]{1,0:T(8,128)} fusion(bf16[64,1024]{1,0:T(8,128)(2,1)S(1)} %bitcast.84, bf16[1024,256]{1,0:T(8,128)(2,1)} %param.23, bf16[1024,256]{1,0:T(8,128)(2,1)} %param.22, bf16[1024,256]{1,0:T(8,128)(2,1)} %param.21), kind=kOutput, calls=%fused_computation.16 | convolution fusion | flops 105381888 | bytes 1900544 | tf_op jit(solution)/shard_map/dot_general | solution.py:46
  22.8 0.1 iota_compare_fusion
  22.9 12.3 %copy.74 = bf16[16,1024,256]{1,2,0:T(8,128)(2,1)} copy(bf16[16,1024,256]{2,1,0:T(8,128)(2,1)} %param.27) | data formatting | bytes 16777216 | tf_op args[8]
  35.2 0.1 copy.79
  35.3 0.1 broadcast_multiply_fusion
  35.4 11.5 %reduce-scatter.3.cloned.1.call-done = f32[16,768]{1,0:T(8,128)} async-done(((f32[64,768]{1,0:T(8,128)}), f32[16,768]{1,0:T(8,128)}) %reduce-scatter.3.cloned.1.call-update) | async-done | bytes 49168 | tf_op jit(solution)/shard_map/reduce_scatter | solution.py:45
  46.9 0.8 convert_element_type.87
  47.7 0.1 reshape.176
  47.8 0.1 reshape.201
  47.9 0.1 reshape.187
  48.0 0.1 multiply_reduce_fusion.2
  48.1 0.1 copy.75
  48.2 4.6 %fusion.3 = f32[2,16,2,1,1024]{4,3,2,1,0:T(1,128)S(1)} fusion(bf16[16,1024,2,2,64]{1,4,3,2,0:T(8,128)(2,1)} %bitcast.81, bf16[16,2,2,64,1]{3,2,1,0,4:T(2,128)(2,1)S(1)} %reshape.201), kind=kOutput, calls=%fused_computation.4 | convolution fusion | flops 8388608 | bytes 8658944 | tf_op jit(solution)/shard_map/shcd,slhcd->cshl/dot_general | solution.py:65
  52.8 0.2 fusion.66
  53.0 0.1 copy.76
  53.1 0.8 fusion.35
  53.9 0.1 fusion.39
  54.1 0.2 copy.89
  54.3 4.7 %fusion = f32[16,2,1,128]{3,2,1,0:T(1,128)S(1)} fusion(bf16[16,2,1024,1]{2,0,1,3:T(8,128)(2,1)S(1)} %slice_bitcast_fusion.2, bf16[16,1024,256]{2,1,0:T(8,128)(2,1)} %param.28), kind=kOutput, calls=%fused_computation.1 | convolution fusion | flops 8388608 | bytes 8470528 | tf_op jit(solution)/shard_map/shl,slhe->she/dot_general | solution.py:74
  59.0 0.2 multiply_reduce_fusion.3
  59.2 0.1 multiply_convert_fusion.2
  59.3 1.0 convolution_convert_fusion.2
  60.5 55.0 %all-reduce.2.cloned.1.call-done = bf16[16,4096]{1,0:T(8,128)(2,1)} async-done(((bf16[16,4096]{1,0:T(8,128)(2,1)}), bf16[16,4096]{1,0:T(8,128)(2,1)}) %all-reduce.2.cloned.1.call-update) | async-done | bytes 131088 | tf_op jit(solution)/shard_map/psum | solution.py:86
  115.5 1.1 convert_add_fusion
  116.6 1.2 fusion.5
  117.8 9.2 %all_to_all.37 = bf16[4,1,8,4096]{3,2,1,0:T(8,128)(2,1)S(1)} all-to-all(bf16[4,1,8,4096]{3,2,1,0:T(8,128)(2,1)S(1)} %fusion.5), channel_id=1, replica_groups=mesh['ep'=4,'tp'=8] {'ep'}, dimensions={0} | all-to-all | bytes 524288 | tf_op jit(solution)/shard_map/all_to_all | solution.py:108
  126.9 2.0 %fusion.10 = f32[32,256]{1,0:T(8,128)S(1)} fusion(bf16[1,4096,256]{2,1,0:T(8,128)(2,1)} %param.35, bf16[4,1,8,4096]{3,2,1,0:T(8,128)(2,1)S(1)} %all_to_all.37), kind=kOutput, calls=%fused_computation.14 | convolution fusion | flops 67108864 | bytes 2392064 | tf_op jit(solution)/shard_map/erd,edf->erf/dot_general | solution.py:110
  129.0 3.6 %fusion.6 = bf16[1,32,4096]{2,1,0:T(8,128)(2,1)} fusion(bf16[1,256,4096]{2,1,0:T(8,128)(2,1)S(1)} %copy-done, bf16[1,4096,256]{2,1,0:T(8,128)(2,1)} %param.36, bf16[4,1,8,4096]{3,2,1,0:T(8,128)(2,1)S(1)} %all_to_all.37, f32[32,256]{1,0:T(8,128)S(1)} %fusion.10), kind=kOutput, calls=%fused_computation.9 | convolution fusion | flops 134397952 | bytes 4751360 | tf_op jit(solution)/shard_map/erf,efd->erd/dot_general | solution.py:113
  132.6 0.1 reshape.192
  132.8 28.4 %reduce-scatter.5.cloned.1.call-done = bf16[1,32,512]{2,1,0:T(8,128)(2,1)} async-done(((bf16[1,32,4096]{2,1,0:T(8,128)(2,1)}), bf16[1,32,512]{2,1,0:T(8,128)(2,1)}) %reduce-scatter.5.cloned.1.call-update) | async-done | bytes 32784 | tf_op jit(solution)/shard_map/reduce_scatter | solution.py:114
  161.1 3.7 %all-to-all-start.2 = ((bf16[1,4,8,512]{3,2,0,1:T(8,128)(2,1)}), bf16[1,4,8,512]{3,2,0,1:T(8,128)(2,1)S(1)}, u32[]{:S(2)}, u32[]{:S(2)}) async-start(bf16[1,4,8,512]{3,2,0,1:T(8,128)(2,1)} %bitcast.90), calls=%async_computation.4 | async-start | bytes 65536 | tf_op jit(solution)/shard_map/all_to_all | solution.py:116
  164.8 0.1 copy.82
  164.9 4.7 %all-to-all-done.2 = bf16[1,4,8,512]{3,2,0,1:T(8,128)(2,1)S(1)} async-done(((bf16[1,4,8,512]{3,2,0,1:T(8,128)(2,1)}), bf16[1,4,8,512]{3,2,0,1:T(8,128)(2,1)S(1)}, u32[]{:S(2)}, u32[]{:S(2)}) %all-to-all-start.2) | async-done | bytes 32800 | tf_op jit(solution)/shard_map/all_to_all | solution.py:116
  169.5 0.6 gather_fusion
  170.2 0.1 multiply_reduce_fusion.1
  170.4 0.6 add_convert_fusion
  (48 shorter events, 0.7 us)
Async XLA Ops:
  7.2 121.8 %copy-start = (bf16[1,256,4096]{2,1,0:T(8,128)(2,1)S(1)}, bf16[1,256,4096]{2,1,0:T(8,128)(2,1)}, u32[]{:S(2)}) copy-start(bf16[1,256,4096]{2,1,0:T(8,128)(2,1)} %param.37) | copy-start | bytes 6291460
  10.0 10.2 %all-to-all-start = ((bf16[16,4,1024]{2,0,1:T(8,128)(2,1)}), bf16[16,4,1024]{2,0,1:T(8,128)(2,1)S(1)}, u32[]{:S(2)}, u32[]{:S(2)}) async-start(bf16[16,4,1024]{2,0,1:T(8,128)(2,1)} %bitcast.80), calls=%async_computation | async-start | bytes 262144 | tf_op jit(solution)/shard_map/all_to_all | solution.py:44
  15.2 31.7 %reduce-scatter.3.cloned.1.call-start = ((), (), s32[]{:S(2)}) async-start(), calls=%async_computation.5 | async-start | bytes 245760 | tf_op jit(solution)/shard_map/reduce_scatter | solution.py:45
  20.3 2.6 %copy-start.7 = (s32[16]{0:T(128)S(1)}, s32[16]{0:T(128)}, u32[]{:S(2)}) copy-start(s32[16]{0:T(128)} %param.29) | copy-start | bytes 196
  22.8 92.7 %all-reduce.2.cloned.1.call-start = ((), (), s32[]{:S(2)}) async-start(), calls=%async_computation.6 | async-start | bytes 262144 | tf_op jit(solution)/shard_map/psum | solution.py:86
  47.7 5.1 %copy-start.4 = (bf16[16,256]{1,0:T(8,128)(2,1)}, bf16[16,256]{1,0:T(8,128)(2,1)S(1)}, u32[]{:S(2)}) copy-start(bf16[16,256]{1,0:T(8,128)(2,1)S(1)} %get-tuple-element.10) | copy-start | bytes 24580
  47.7 6.5 %copy-start.3 = (bf16[16,256]{1,0:T(8,128)(2,1)}, bf16[16,256]{1,0:T(8,128)(2,1)S(1)}, u32[]{:S(2)}) copy-start(bf16[16,256]{1,0:T(8,128)(2,1)S(1)} %get-tuple-element.9) | copy-start | bytes 24580
  52.8 1.1 copy-start.8
  54.3 4.9 %copy-start.9 = (f32[128]{0:T(128)S(1)}, f32[128]{0:T(128)}, u32[]{:S(2)}) copy-start(f32[128]{0:T(128)} %param.25) | copy-start | bytes 1540
  54.3 5.0 %copy-start.2 = (bf16[256,4096]{1,0:T(8,128)(2,1)S(1)}, bf16[256,4096]{1,0:T(8,128)(2,1)}, u32[]{:S(2)}) copy-start(bf16[256,4096]{1,0:T(8,128)(2,1)} %param.26) | copy-start | bytes 6291460
  59.0 56.5 %copy-start.1 = (bf16[16,4096]{1,0:T(8,128)(2,1)S(1)}, bf16[16,4096]{1,0:T(8,128)(2,1)}, u32[]{:S(2)}) copy-start(bf16[16,4096]{1,0:T(8,128)(2,1)} %param.19) | copy-start | bytes 393220
  59.0 57.5 %copy-start.5 = (f32[4096]{0:T(1024)S(1)}, f32[4096]{0:T(1024)}, u32[]{:S(2)}) copy-start(f32[4096]{0:T(1024)} %param.30) | copy-start | bytes 49156
  60.4 100.7 %reduce-scatter.5.cloned.1.call-start = ((), (), s32[]{:S(2)}) async-start(), calls=%async_computation.7 | async-start | bytes 294912 | tf_op jit(solution)/shard_map/reduce_scatter | solution.py:114
  129.0 3.7 %copy-start.6 = (f32[16,2]{0,1:T(2,128)S(1)}, f32[16,2]{0,1:T(2,128)}, u32[]{:S(2)}) copy-start(f32[16,2]{0,1:T(2,128)} %param.34) | copy-start | bytes 388
  129.0 3.8 %copy-start.10 = (f32[16]{0:T(128)S(1)}, f32[16]{0:T(128)}, u32[]{:S(2)}) copy-start(f32[16]{0:T(128)} %param.33) | copy-start | bytes 196
  161.1 8.4 %all-to-all-start.2 = ((bf16[1,4,8,512]{3,2,0,1:T(8,128)(2,1)}), bf16[1,4,8,512]{3,2,0,1:T(8,128)(2,1)S(1)}, u32[]{:S(2)}, u32[]{:S(2)}) async-start(bf16[1,4,8,512]{3,2,0,1:T(8,128)(2,1)} %bitcast.90), calls=%async_computation.4 | async-start | bytes 65536 | tf_op jit(solution)/shard_map/all_to_all | solution.py:116
Sparse Core Ops, SparseCore 0:
  22.9 23.9 reduce-scatter.2
  60.5 54.9 all-reduce.1
  132.7 28.3 reduce-scatter.4
where the time goes:
time: 178 us
  waiting for transfers between devices  102 us (57%)
  matrix products  19.6 us (11%)
  local copies, waits for them, and re-layouts  15.5 us (9%)
  between operations  14 us (8%)
  blocking collectives  9.17 us (5%)
  starting transfers between devices  8.93 us (5%)
  other arithmetic  8.5 us (5%)
    psum x1, waiting for transfers between devices, on_device(): lax.psum(lax.optimization_barrier(term).astype(jnp.float32).astype(jnp.bf...  55 us
    reduce_scatter x1, waiting for transfers between devices, on_device(): lax.psum_scatter(down.astype(jnp.bfloat16), 'tp', scatter_dimension=2, ti...  28.4 us
    unnamed x24, local copies, waits for them, and re-layouts  13.1 us
    reduce_scatter x1, waiting for transfers between devices, on_device(): lax.psum_scatter(jnp.dot(sliced, stacked, preferred_element_type=jnp.floa...  11.5 us
    all_to_all x1, blocking collectives, on_device(): lax.all_to_all(dispatch, 'ep', split_axis=0, concat_axis=2, tiled=True)  9.17 us
    all_to_all x1, starting transfers between devices, on_device(): lax.all_to_all(normed, 'ep', split_axis=1, concat_axis=0, tiled=True)  5.19 us
    dot_general x1, matrix products, on_device(): jnp.einsum('shl,slhe->she', weights[..., :positions_all], values, preferr...  4.72 us
    all_to_all x1, waiting for transfers between devices, on_device(): lax.all_to_all(summed.reshape(experts_local, ep_count, capacity, cols), '...  4.66 us
  transfers between devices with their start and end apart: 5, of which 5 were waited for; matrix products, arithmetic and copies ran while one was open for 9% of the time, Pallas kernels for 0%

commit v1 on v0

v1 whole, which is shorter than its diff:
```python
import functools

import jax
import jax.numpy as jnp
from jax import lax
from jax.experimental import pallas as pl
from jax.experimental.pallas import tpu as pltpu
from jax.sharding import PartitionSpec as P

EPG = 2
EPS = 1e-06
MESH = pl.DeviceIdType.MESH
F32 = jnp.float32
BF16 = jnp.bfloat16
GROUP = 4


def iota(shape, dim):
    return lax.broadcasted_iota(jnp.int32, shape, dim)


def layer_kernel(
    n_ep, n_tp, cap,
    tokens, attn_gain, head_gain, moe_gain, lam, lengths, eids, group_gate, logits,
    w_query, w_key, w_value, cache_keys, cache_value, w_output, w_gate, w_up, w_down,
    mixed, fresh_keys, fresh_value,
    wq, wk, wv, kbuf, vbuf, wo, wg, wu, wd,
    nsend, nrecv, psend, precv, query, fkey, fval, head_out,
    tsend, trecv, qsend, qrecv, dsend, drecv, csend, crecv,
    w_sem, c_sem, n_ss, n_rs, p_ss, p_rs, t_ss, t_rs, q_ss, q_rs, d_ss, d_rs, e_ss, e_rs,
):
    ep = lax.axis_index("ep")
    tp = lax.axis_index("tp")
    devices = n_ep * n_tp
    me = ep * n_tp + tp
    seqs, width = tokens.shape
    rows_local = width // n_ep
    qk_cols = w_query.shape[1]
    heads_local = lam.shape[0]
    pair = qk_cols // heads_local
    head_dim = pair // 2
    total_heads = heads_local * n_tp
    positions = cache_keys.shape[1]
    cols = width // n_tp
    slot_rows = dsend.shape[1]
    slots = n_ep * slot_rows

    barrier = pltpu.get_barrier_semaphore()

    def greet(d, carry):
        other = lax.rem(me + d, devices)
        pl.semaphore_signal(
            barrier, inc=1, device_id={"ep": other // n_tp, "tp": lax.rem(other, n_tp)}, device_id_type=MESH
        )
        return carry

    lax.fori_loop(1, devices, greet, 0)

    weight_pairs = [(w_query, wq), (w_key, wk), (w_value, wv), (w_output, wo), (w_gate, wg), (w_up, wu), (w_down, wd)]

    def weight_copy(i):
        return pltpu.make_async_copy(weight_pairs[i][0], weight_pairs[i][1], w_sem.at[i])

    def cache_copy(g, kind):
        src, dst = ((cache_keys, kbuf), (cache_value, vbuf))[kind]
        rows = pl.ds(g * GROUP, GROUP)
        return pltpu.make_async_copy(src.at[rows], dst.at[rows], c_sem.at[kind, g])

    for i in range(3):
        weight_copy(i).start()
    for g in range(seqs // GROUP):
        cache_copy(g, 0).start()
        cache_copy(g, 1).start()
    for i in range(3, 7):
        weight_copy(i).start()

    resid_in = tokens[...].astype(F32)
    inv = lax.rsqrt(jnp.mean(resid_in * resid_in, axis=-1, keepdims=True) + EPS)
    normed = (resid_in * inv * attn_gain[...]).astype(BF16)
    for e in range(n_ep):
        nsend[e] = normed[:, e * rows_local : (e + 1) * rows_local]
    nrecv[ep] = nsend[ep]

    pl.semaphore_wait(barrier, devices - 1)

    def over_ep(send, recv, ss, rs, d):
        other = lax.rem(ep + d, n_ep)
        return pltpu.make_async_remote_copy(
            src_ref=send.at[other], dst_ref=recv.at[ep], send_sem=ss.at[d], recv_sem=rs.at[d],
            device_id={"ep": other, "tp": tp}, device_id_type=MESH,
        )

    for d in range(1, n_ep):
        over_ep(nsend, nrecv, n_ss, n_rs, d).start()
    for i in range(3):
        weight_copy(i).wait()
    for d in range(1, n_ep):
        over_ep(nsend, nrecv, n_ss, n_rs, d).wait_recv()
    rows_all = nrecv[...].reshape(n_ep * seqs, rows_local)
    for i, w in enumerate((wq, wk, wv)):
        part = jnp.dot(rows_all, w[...], preferred_element_type=F32)
        psend[:, :, i * qk_cols : (i + 1) * qk_cols] = part.reshape(n_ep, seqs, qk_cols)
    for d in range(1, n_ep):
        over_ep(psend, precv, p_ss, p_rs, d).start()
    precv[ep] = psend[ep]

    slot = iota((seqs, slots), 1)
    expert_of = slot // slot_rows
    rank_of = (slot % slot_rows).astype(F32)
    hits = [eids[:, k : k + 1] == expert_of for k in range(2)]
    used = (hits[0] | hits[1]).astype(BF16)
    lower = (iota((seqs, seqs), 1) < iota((seqs, seqs), 0)).astype(BF16)
    ranks = jnp.dot(lower, used, preferred_element_type=F32)
    in_slot = ranks == rank_of
    chosen = [(hits[k] & in_slot).astype(F32) for k in range(2)]
    picker = (chosen[0] + chosen[1]).T.astype(BF16)
    lg = logits[...]
    ex = jnp.exp(lg - jnp.max(lg, axis=-1, keepdims=True))
    route = ex / jnp.sum(ex, axis=-1, keepdims=True) * group_gate[...]

    for d in range(1, n_ep):
        over_ep(psend, precv, p_ss, p_rs, d).wait_recv()
    total = precv[0]
    for e in range(1, n_ep):
        total = total + precv[e]
    projected = total.astype(BF16)
    fresh_keys[...] = projected[:, qk_cols : 2 * qk_cols]
    fresh_value[...] = projected[:, 2 * qk_cols :]
    projected = projected.astype(F32)
    query[...] = projected[:, :qk_cols]
    fkey[...] = projected[:, qk_cols : 2 * qk_cols]
    fval[...] = projected[:, 2 * qk_cols :]

    scale = head_dim ** (-0.5)
    row16 = iota((16, qk_cols), 0)
    col16 = iota((16, qk_cols), 1)
    map_mask = ((col16 // pair == row16 % 8) & ((col16 // head_dim) % 2 == row16 // 8)).astype(F32)
    head_mask = (iota((8, qk_cols), 1) // pair == iota((8, qk_cols), 0)).astype(F32)
    head_row = (tp * heads_local + iota((16, 1), 0) % 8).astype(F32)
    slopes = jnp.exp2(-8.0 * (head_row + 1.0) / total_heads)
    lam_col = jnp.zeros((8, 1), F32)
    for h in range(heads_local):
        lam_col = jnp.where(iota((8, 1), 0) == h, lam[h], lam_col)
    gain_row = jnp.concatenate([head_gain[...]] * heads_local, axis=1)
    spots = iota((1, positions), 1)

    def attend(g, carry):
        cache_copy(g, 0).wait()
        cache_copy(g, 1).wait()
        olds, news = [], []
        for i in range(GROUP):
            s = g * GROUP + i
            q16 = query[pl.ds(s, 1), :] * map_mask
            old = lax.dot_general(
                q16.astype(BF16), kbuf[s], (((1,), (1,)), ((), ())), preferred_element_type=F32
            )
            n = lengths[s]
            old = old * scale - slopes * (n - spots).astype(F32)
            olds.append(jnp.where(spots < n, old, -jnp.inf))
            news.append(jnp.sum(q16 * fkey[pl.ds(s, 1), :], axis=-1, keepdims=True) * scale)
        for i in range(GROUP):
            s = g * GROUP + i
            top = jnp.maximum(jnp.max(olds[i], axis=-1, keepdims=True), news[i])
            old = jnp.exp(olds[i] - top)
            new = jnp.exp(news[i] - top)
            recip = 1.0 / (jnp.sum(old, axis=-1, keepdims=True) + new)
            old = old * recip
            new = new * recip
            weights = (old[:8] - lam_col * old[8:]).astype(BF16)
            fresh = (new[:8] - lam_col * new[8:]).astype(BF16).astype(F32)
            mix = jnp.dot(weights, vbuf[s], preferred_element_type=F32)
            mix = (mix + fresh * fval[pl.ds(s, 1), :]) * head_mask
            mean = jnp.sum(mix * mix, axis=-1, keepdims=True) / pair
            mix = mix * lax.rsqrt(mean + EPS) * gain_row
            head_out[pl.ds(s, 1), :] = jnp.sum(mix, axis=0, keepdims=True)
        return carry

    lax.fori_loop(0, seqs // GROUP, attend, 0)

    weight_copy(3).wait()
    heads = head_out[...].astype(BF16)
    for t in range(n_tp):
        tsend[t] = jnp.dot(
            heads, wo[:, t * cols : (t + 1) * cols], preferred_element_type=F32
        ).astype(BF16)

    def over_tp(send, recv, ss, rs, d, same=False):
        other = lax.rem(tp + d, n_tp)
        return pltpu.make_async_remote_copy(
            src_ref=send if same else send.at[other], dst_ref=recv.at[tp], send_sem=ss.at[d], recv_sem=rs.at[d],
            device_id={"ep": ep, "tp": other}, device_id_type=MESH,
        )

    for d in range(1, n_tp):
        over_tp(tsend, trecv, t_ss, t_rs, d).start()
    trecv[tp] = tsend[tp]
    for d in range(1, n_tp):
        over_tp(tsend, trecv, t_ss, t_rs, d).wait_recv()
    attn = trecv[0].astype(F32)
    for t in range(1, n_tp):
        attn = attn + trecv[t].astype(F32)
    my_cols = pl.ds(pl.multiple_of(tp * cols, cols), cols)
    resid = tokens[:, my_cols].astype(F32) + attn
    squares = jnp.sum(resid * resid, axis=-1, keepdims=True)
    qsend[...] = jnp.broadcast_to(squares, qsend.shape)
    for d in range(1, n_tp):
        over_tp(qsend, qrecv, q_ss, q_rs, d, True).start()
    qrecv[tp] = qsend[...]
    for d in range(1, n_tp):
        over_tp(qsend, qrecv, q_ss, q_rs, d, True).wait_recv()
    squares = qrecv[0]
    for t in range(1, n_tp):
        squares = squares + qrecv[t]
    inv = lax.rsqrt(squares[:, :1] / width + EPS)
    moe_in = (resid * inv * moe_gain[:, my_cols]).astype(BF16)
    dispatch = jnp.dot(picker, moe_in, preferred_element_type=F32)
    for e in range(n_ep):
        dsend[e] = dispatch[e * slot_rows : (e + 1) * slot_rows].astype(BF16)

    def spread(d):
        other = lax.rem(me + d, devices)
        other_ep, other_tp = other // n_tp, lax.rem(other, n_tp)
        return pltpu.make_async_remote_copy(
            src_ref=dsend.at[other_ep], dst_ref=drecv.at[tp, ep], send_sem=d_ss.at[d], recv_sem=d_rs.at[d],
            device_id={"ep": other_ep, "tp": other_tp}, device_id_type=MESH,
        )

    def gather(d):
        other = lax.rem(me + d, devices)
        other_ep, other_tp = other // n_tp, lax.rem(other, n_tp)
        return pltpu.make_async_remote_copy(
            src_ref=csend.at[other_tp, other_ep], dst_ref=crecv.at[tp, ep], send_sem=e_ss.at[d], recv_sem=e_rs.at[d],
            device_id={"ep": other_ep, "tp": other_tp}, device_id_type=MESH,
        )

    def each(action):
        def step(d, carry):
            action(d)
            return carry

        lax.fori_loop(1, devices, step, 0)

    each(lambda d: spread(d).start())
    drecv[tp, ep] = dsend[ep]
    weight_copy(4).wait()
    weight_copy(5).wait()
    each(lambda d: spread(d).wait_recv())
    gate = jnp.zeros((slots, w_gate.shape[2]), F32)
    upper = gate
    for t in range(n_tp):
        rows = drecv[t].astype(F32).reshape(slots, cols).astype(BF16)
        gate = gate + jnp.dot(rows, wg[0, t * cols : (t + 1) * cols], preferred_element_type=F32)
        upper = upper + jnp.dot(rows, wu[0, t * cols : (t + 1) * cols], preferred_element_type=F32)
    hidden = (gate / (1.0 + jnp.exp(-gate)) * upper).astype(BF16)
    weight_copy(6).wait()
    for t in range(n_tp):
        down = jnp.dot(hidden, wd[0, :, t * cols : (t + 1) * cols], preferred_element_type=F32)
        csend[t] = down.reshape(n_ep, slot_rows, cols).astype(BF16)
    each(lambda d: gather(d).start())
    crecv[tp, ep] = csend[tp, ep]
    each(lambda d: gather(d).wait_recv())
    out = crecv[0].astype(F32)
    for t in range(1, n_tp):
        out = out + crecv[t].astype(F32)
    out = out.reshape(slots, cols).astype(BF16)
    routed = jnp.zeros((seqs, cols), F32)
    for k in range(2):
        picked = jnp.dot(chosen[k].astype(BF16), out, preferred_element_type=F32)
        routed = routed + route[:, k : k + 1] * picked
    mixed[...] = (resid + routed).astype(BF16)

    for d in range(1, n_ep):
        over_ep(nsend, nrecv, n_ss, n_rs, d).wait_send()
        over_ep(psend, precv, p_ss, p_rs, d).wait_send()
    for d in range(1, n_tp):
        over_tp(tsend, trecv, t_ss, t_rs, d).wait_send()
        over_tp(qsend, qrecv, q_ss, q_rs, d, True).wait_send()
    each(lambda d: spread(d).wait_send())
    each(lambda d: gather(d).wait_send())


def on_device(
    tokens, attn_gain, w_query, w_key, w_value, mix_lambda, head_gain, w_output, cache_keys, cache_value,
    lengths, moe_gain, group_ids, member_ids, group_gate, member_logits, w_exp_gate, w_exp_up, w_exp_down,
):
    n_ep, n_tp = lax.axis_size("ep"), lax.axis_size("tp")
    seqs, width = tokens.shape
    qk_cols = w_query.shape[1]
    experts_all = w_exp_gate.shape[0] * n_ep
    cap = seqs * member_ids.shape[1] // experts_all
    slot_rows = -(-cap // 8) * 8
    cols = width // n_tp
    devices = n_ep * n_tp
    eids = group_ids[:, None] * EPG + member_ids
    vmem = pl.BlockSpec(memory_space=pltpu.VMEM)
    smem = pl.BlockSpec(memory_space=pltpu.SMEM)
    hbm = pl.BlockSpec(memory_space=pl.ANY)
    dma = pltpu.SemaphoreType.DMA
    like = lambda a: pltpu.VMEM(a.shape, a.dtype)
    scratch = [
        like(w_query), like(w_key), like(w_value), like(cache_keys), like(cache_value),
        like(w_output), like(w_exp_gate), like(w_exp_up), like(w_exp_down),
        pltpu.VMEM((n_ep, seqs, width // n_ep), BF16),
        pltpu.VMEM((n_ep, seqs, width // n_ep), BF16),
        pltpu.VMEM((n_ep, seqs, 3 * qk_cols), F32),
        pltpu.VMEM((n_ep, seqs, 3 * qk_cols), F32),
        pltpu.VMEM((seqs, qk_cols), F32),
        pltpu.VMEM((seqs, qk_cols), F32),
        pltpu.VMEM((seqs, qk_cols), F32),
        pltpu.VMEM((seqs, qk_cols), F32),
        pltpu.VMEM((n_tp, seqs, cols), BF16),
        pltpu.VMEM((n_tp, seqs, cols), BF16),
        pltpu.VMEM((seqs, 128), F32),
        pltpu.VMEM((n_tp, seqs, 128), F32),
        pltpu.VMEM((n_ep, slot_rows, cols), BF16),
        pltpu.VMEM((n_tp, n_ep, slot_rows, cols), BF16),
        pltpu.VMEM((n_tp, n_ep, slot_rows, cols), BF16),
        pltpu.VMEM((n_tp, n_ep, slot_rows, cols), BF16),
        dma((7,)), dma((2, seqs // GROUP)),
        dma((n_ep,)), dma((n_ep,)), dma((n_ep,)), dma((n_ep,)),
        dma((n_tp,)), dma((n_tp,)), dma((n_tp,)), dma((n_tp,)),
        dma((devices,)), dma((devices,)), dma((devices,)), dma((devices,)),
    ]
    return pl.pallas_call(
        functools.partial(layer_kernel, n_ep, n_tp, cap),
        out_shape=(
            jax.ShapeDtypeStruct((seqs, cols), BF16),
            jax.ShapeDtypeStruct((seqs, qk_cols), BF16),
            jax.ShapeDtypeStruct((seqs, qk_cols), BF16),
        ),
        in_specs=[vmem] * 4 + [smem] * 2 + [vmem] * 3 + [hbm] * 9,
        out_specs=(vmem, vmem, vmem),
        scratch_shapes=scratch,
        compiler_params=pltpu.CompilerParams(
            collective_id=0, has_side_effects=True, vmem_limit_bytes=60 * 1024 * 1024
        ),
        name="decode_layer",
    )(
        tokens, attn_gain[None, :], head_gain[None, :], moe_gain[None, :], mix_lambda, lengths,
        eids, group_gate[:, None], member_logits,
        w_query, w_key, w_value, cache_keys, cache_value, w_output, w_exp_gate, w_exp_up, w_exp_down,
    )


def solution(mesh):
    return jax.shard_map(
        on_device,
        mesh=mesh,
        in_specs=(
            P("ep", None),
            P(),
            P("ep", "tp"),
            P("ep", "tp"),
            P("ep", "tp"),
            P("tp"),
            P(),
            P("tp", None),
            P("ep", None, "tp"),
            P("ep", None, "tp"),
            P("ep"),
            P(),
            P("ep"),
            P("ep", None),
            P("ep"),
            P("ep", None),
            P("ep", None, "tp"),
            P("ep", None, "tp"),
            P("ep", "tp", None),
        ),
        out_specs=(P("ep", "tp"), P("ep", "tp"), P("ep", "tp")),
        check_vma=False,
    )
```

time: 178 us -> 58.6 us (0.33)
  waiting for transfers between devices: 102 us -> 0 us
  Pallas kernels: 0 us -> 48.9 us
  matrix products: 19.6 us -> 0 us
  between operations: 14 us -> 0.64 us
  blocking collectives: 9.17 us -> 0 us
  starting transfers between devices: 8.93 us -> 0 us
  local copies, waits for them, and re-layouts: 15.5 us -> 7.35 us
  other arithmetic: 8.5 us -> 1.33 us
    psum x1 -> x0, waiting for transfers between devices: 55 us -> none  [on_device(): lax.psum(lax.optimization_barrier(term).astype(jnp.float32).astype(jnp.bf...]
    pallas_call x0 -> x1, Pallas kernels: none -> 48.9 us  [on_device(): pl.pallas_call(functools.partial(layer_kernel, n_ep, n_tp, cap), out_shap...]
    reduce_scatter x2 -> x0, waiting for transfers between devices: 39.9 us -> none  [the longest x1 28.4 us: on_device(): lax.psum_scatter(down.astype(jnp.bfloat16), 'tp', scatter_dimension=2, ti...]
    dot_general x7 -> x0, matrix products: 19.6 us -> none  [the longest x1 4.72 us: on_device(): jnp.einsum('shl,slhe->she', weights[..., :positions_all], values, preferr...]
    all_to_all x1 -> x0, blocking collectives: 9.17 us -> none  [on_device(): lax.all_to_all(dispatch, 'ep', split_axis=0, concat_axis=2, tiled=True)]
    all_to_all x2 -> x0, starting transfers between devices: 8.84 us -> none  [the longest x1 5.19 us: on_device(): lax.all_to_all(normed, 'ep', split_axis=1, concat_axis=0, tiled=True)]
    unnamed x24 -> x5, local copies, waits for them, and re-layouts: 13.1 us -> 6.02 us
    all_to_all x2 -> x0, waiting for transfers between devices: 6.89 us -> none  [the longest x1 4.66 us: on_device(): lax.all_to_all(summed.reshape(experts_local, ep_count, capacity, cols), '...]
  transfers between devices with their start and end apart: 5 -> 0, of which waited for: 5 -> 0; matrix products, arithmetic and copies ran while one was open for 9% -> 0% of each run, Pallas kernels for 0% -> 0%
where the time goes in v1:
time: 58.6 us; the launch traced here: 58.2 us
  Pallas kernels  48.9 us (83%)
  local copies, waits for them, and re-layouts  7.35 us (13%)
  other arithmetic  1.33 us (2%)
  between operations  0.64 us (1%)
    pallas_call x1, Pallas kernels, on_device(): pl.pallas_call(functools.partial(layer_kernel, n_ep, n_tp, cap), out_shap...  48.9 us
    unnamed x5, local copies, waits for them, and re-layouts  6.02 us
    broadcast_in_dim x1, local copies, waits for them, and re-layouts, on_device(): group_gate[:, None]  1.33 us

profile of v1, /device:TPU:0, one launch (start us, length us, event | category | flops | bytes accessed | tf_op | source)
XLA Modules:
  0.0 58.2 jit_solution(11024290566816431203)
XLA Ops:
  0.6 0.7 %broadcast_multiply_fusion = s32[16]{0:T(128)S(1)} fusion(s32[16]{0:T(128)} %param.31), kind=kLoop, calls=%fused_computation.1 | loop fusion | flops 16 | bytes 128 | tf_op jit(solution)/shard_map/mul | solution.py:294
  1.3 0.8 %copy.26 = s32[16,2]{1,0:T(8,128)S(1)} copy(s32[16,2]{0,1:T(2,128)} %param.32) | data formatting | bytes 256 | tf_op args[13]
  2.0 0.7 %broadcast_add_fusion.eids = s32[16,2]{1,0:T(8,128)} fusion(s32[16,2]{1,0:T(8,128)S(1)} %copy.26, s32[16]{0:T(128)S(1)} %broadcast_multiply_fusion), kind=kLoop, calls=%fused_computation | loop fusion | flops 32 | bytes 320 | tf_op jit(solution)/shard_map/add | solution.py:294
  2.7 1.3 %copy.27.group_gate = f32[16,1]{1,0:T(8,128)} copy(f32[16,1]{0,1:T(1,128)} %bitcast.7) | data formatting | bytes 128 | tf_op jit(solution)/shard_map/broadcast_in_dim | solution.py:340
  4.0 1.4 %copy.28.logits = f32[16,2]{1,0:T(8,128)} copy(f32[16,2]{0,1:T(2,128)} %param.34) | data formatting | bytes 256 | tf_op args[15]
  5.4 48.9 %decode_layer.1 = (bf16[16,512]{1,0:T(8,128)(2,1)}, bf16[16,256]{1,0:T(8,128)(2,1)}, bf16[16,256]{1,0:T(8,128)(2,1)}) custom-call(bf16[16,4096]{1,0:T(8,128)(2,1)} %tokens.1, f32[1,4096]{1,0:T(1,128)} %bitcast.4, f32[1,128]{1,0:T(1,128)} %bitcast.6, f32[1,4096]{1,0:T(1,128)} %bitcast.5, f32[2]{0:T(128)} %lam.1, s32[16]{0:T(128)} %lengths.1, ...), custom_call_target="tpu_custom_call" | custom-call | tf_op jit(solution)/shard_map/decode_layer/pallas_call | solution.py:324
  54.3 1.3 %copy.32 = bf16[16,512]{1,0:T(8,128)(2,1)} copy(bf16[16,512]{1,0:T(8,128)(2,1)} %get-tuple-element.6) | data formatting | bytes 32768
  55.6 1.3 %copy.33 = bf16[16,256]{1,0:T(8,128)(2,1)} copy(bf16[16,256]{1,0:T(8,128)(2,1)} %get-tuple-element.7) | data formatting | bytes 16384
  56.9 1.3 %copy.34 = bf16[16,256]{1,0:T(8,128)(2,1)} copy(bf16[16,256]{1,0:T(8,128)(2,1)} %get-tuple-element.8) | data formatting | bytes 16384
